TPU v7x, 32 devices: a whole 2x2x4 slice. The times are simulated.
32 devices in a mesh: tp: 4 (over y, x), dp: 8 (over z, core).
Axes of the slice: x: 2, y: 2, z: 4, core: 2. Of those that a mesh axis runs over, the one named last changes fastest.
Arguments:
- hidden_vectors: bfloat16 [48, 4096], P('tp', 'dp'), may hold values from -8 to 8
- live_spans: int32 [24], P('dp'), may hold values from 1 to 2, as said below
- entry_rescale: bfloat16 [2, 4096], P(None, 'dp'), may hold values from 0.099609375 to 1.8984375
- query_weights: bfloat16 [2, 4096, 2048], P(None, 'dp', 'tp'), may hold values from -0.09375 to 0.09375
- address_weights: bfloat16 [2, 4096, 2048], P(None, 'dp', 'tp'), may hold values from -0.09375 to 0.09375
- content_weights: bfloat16 [2, 4096, 2048], P(None, 'dp', 'tp'), may hold values from -0.09375 to 0.09375
- fade_weights: bfloat16 [2, 4096, 2048], P(None, 'dp', 'tp'), may hold values from -0.09375 to 0.09375
- learning_speed_weights: bfloat16 [2, 4096, 2048], P(None, 'dp', 'tp'), may hold values from -0.09375 to 0.09375
- exit_valve_weights: bfloat16 [2, 4096, 2048], P(None, 'dp', 'tp'), may hold values from -0.09375 to 0.09375
- feature_fade_ceiling: float32 [2, 2048], P(None, 'tp'), may hold values from 0.02 to 2
- subspace_rescale: float32 [2, 2048], P(None, 'tp'), may hold values from 0.1 to 1.9
- exit_weights: bfloat16 [2, 2048, 4096], P(None, 'tp', 'dp'), may hold values from -0.125 to 0.125
- memories: float32 [2, 24, 32, 64, 64], P(None, 'dp', 'tp'), may hold values from -6 to 6
- extra_log_fade: float32 [2, 48, 32], P(None, 'dp', 'tp'), may hold values from -0.7 to 0
Outputs:
- hidden_out: bfloat16 [48, 4096], P('tp', 'dp')
- new_states: float32 [2, 24, 32, 64, 64], P(None, 'dp', 'tp')
Inputs may be any that keep to these rules, and one draw needn't show every extreme that they name: `live_spans`: live slots of each sequence; some sequence has 2.
All inputs are finite; a program needn't handle non-finite values.
Results may differ from a plain program's by a relative error of at most 0.0075.
Values may be sent and summed in bfloat16 or wider, within the bound.
A program may use at most 64 MiB of HBM per device.

v0:
```python
import functools

import jax
import jax.numpy as jnp
from jax import lax
from jax.experimental import pallas as pl
from jax.experimental.pallas import tpu as pltpu
from jax.sharding import PartitionSpec as P

NORM_EPS = 1e-06
KEY_EPS = 1e-06
GROUP_EPS = 0.00064
PAD = 8
EXTRA = 128
F32 = jnp.float32
BF16 = jnp.bfloat16


def kernel(
    n_tp,
    n_dp,
    x_hbm,
    live_ref,
    gain_hbm,
    w0,
    w1,
    w2,
    w3,
    w4,
    w5,
    ceiling_hbm,
    rescale_hbm,
    exit_hbm,
    memory_hbm,
    fade_hbm,
    out_ref,
    state_hbm,
    wv,
    ev,
    mem,
    gx,
    xs,
    ms,
    pown,
    dsend,
    drecv,
    zsend,
    zrecv,
    pr,
    mbuf,
    psend,
    precv,
    gain_ref,
    ceiling_ref,
    rescale_ref,
    fade_ref,
    s_high,
    s_low,
    load_sem,
    store_sem,
    send_sem,
    recv_sem,
):
    blocks = wv.shape[0]
    feats = x_hbm.shape[1]
    chans = wv.shape[3]
    seqs, heads, size = mem.shape[1], mem.shape[2], mem.shape[3]
    rows = zsend.shape[2]
    steps = rows // seqs
    half = 3 * chans
    nz = n_dp // 2
    per_tp = n_dp // n_tp

    tp = lax.axis_index("tp")
    dp = lax.axis_index("dp")
    z = dp // 2
    core = dp % 2
    other = 1 - core

    def peer(tp_at, dp_at):
        return {"tp": tp_at, "dp": dp_at}

    def tp_to(k):
        return lax.rem(tp + k, n_tp)

    def dp_to(dz, flip):
        return lax.rem(z + dz, nz) * 2 + (other if flip else core)

    def dp_from(dz, flip):
        return lax.rem(z + nz - dz, nz) * 2 + (other if flip else core)

    dp_offsets = [(dz, f) for dz in range(nz) for f in range(2) if (dz, f) != (0, 0)]
    far_first = sorted(dp_offsets, key=lambda o: -min(o[0], nz - o[0]))

    def slot_major(values):
        return jnp.concatenate(
            [
                values[s * steps + t : s * steps + t + 1]
                for t in range(steps)
                for s in range(seqs)
            ],
            axis=0,
        )

    def sequence_major(values):
        return jnp.concatenate(
            [
                values[t * seqs + s : t * seqs + s + 1]
                for s in range(seqs)
                for t in range(steps)
            ],
            axis=0,
        )

    counter = [0]

    def remote(src, dst, to):
        at = counter[0]
        counter[0] += 1
        return pltpu.make_async_remote_copy(
            src_ref=src,
            dst_ref=dst,
            send_sem=send_sem.at[at],
            recv_sem=recv_sem.at[at],
            device_id=to,
            device_id_type=pl.DeviceIdType.MESH,
        )

    weights = (w0, w1, w2, w3, w4, w5)
    loads = {}

    def load(name, src, dst):
        copy = pltpu.make_async_copy(src, dst, load_sem.at[len(loads)])
        copy.start()
        loads[name] = copy

    own_x = pltpu.make_async_copy(x_hbm, gx.at[tp], load_sem.at[load_sem.shape[0] - 1])
    own_x.start()
    load("gain", gain_hbm, gain_ref)
    load("ceiling", ceiling_hbm, ceiling_ref)
    load("rescale", rescale_hbm, rescale_ref)
    load("fade", fade_hbm, fade_ref)
    for b in range(blocks):
        for p in range(6):
            load(("w", b, p), weights[p].at[b], wv.at[b, p])
        load(("m", b), memory_hbm.at[b], mem.at[b])
        load(("e", b), exit_hbm.at[b], ev.at[b])

    barrier = pltpu.get_barrier_semaphore()
    for k in range(1, n_tp):
        pl.semaphore_signal(
            barrier, inc=1, device_id=peer(tp_to(k), dp), device_id_type=pl.DeviceIdType.MESH
        )
    for dz, f in dp_offsets:
        pl.semaphore_signal(
            barrier, inc=1, device_id=peer(tp, dp_to(dz, f)), device_id_type=pl.DeviceIdType.MESH
        )
    xs[...] = jnp.zeros_like(xs)
    ms[...] = jnp.zeros_like(ms)
    pr[...] = jnp.zeros_like(pr)
    own_x.wait()
    pl.semaphore_wait(barrier, n_tp - 1 + len(dp_offsets))

    outgoing = []

    first = []
    for k in range(1, n_tp):
        copy = remote(gx.at[tp], gx.at[tp], peer(tp_to(k), dp))
        copy.start()
        first.append(copy)
    for copy in first:
        copy.wait_recv()
    outgoing += first
    for i in range(n_tp):
        whole = gx[i].astype(F32)
        for g in range(per_tp):
            xs[(i * per_tp + g) * PAD : (i * per_tp + g) * PAD + rows, :] = slot_major(
                whole[g * rows : (g + 1) * rows]
            )
    for name in ("gain", "ceiling", "rescale", "fade"):
        loads[name].wait()

    row_at = lax.broadcasted_iota(jnp.int32, (PAD, 1), 0)
    live_col = jnp.zeros((PAD, 1), F32)
    for s in range(seqs):
        for t in range(steps):
            live_col = jnp.where(
                row_at == t * seqs + s, jnp.where(live_ref[s] > t, 1.0, 0.0), live_col
            )
    live3 = [
        live_col[t * seqs : (t + 1) * seqs].reshape(1, seqs, 1) for t in range(steps)
    ]
    extra_at = lax.broadcasted_iota(jnp.int32, (1, EXTRA), 1)

    for b in range(blocks):
        x_now = xs[...]
        gained = (x_now * gain_ref[b : b + 1, :].astype(F32)).astype(BF16)
        squares = jnp.sum(x_now * x_now, axis=1, keepdims=True)
        for p in range(6):
            loads[("w", b, p)].wait()

        high = squares.astype(BF16).astype(F32)
        split = jnp.where(extra_at < EXTRA // 2, high, squares - high)
        for j in range(n_dp):
            dsend[b, j, :, half : half + EXTRA] = split[j * PAD : j * PAD + rows].astype(BF16)
        piece = [pl.ds(p * chans, chans + (EXTRA if p == 2 else 0)) for p in range(3)]
        pairs = []
        for p in range(3):
            part = jnp.dot(gained, wv[b, 3 * other + p], preferred_element_type=F32)
            for j in range(n_dp):
                dsend[b, j, :, p * chans : (p + 1) * chans] = part[
                    j * PAD : j * PAD + rows
                ].astype(BF16)
            pair = remote(
                dsend.at[b, :, :, piece[p]], drecv.at[b, :, :, piece[p]], peer(tp, dp_to(0, 1))
            )
            pair.start()
            pairs.append(pair)
        outgoing += pairs
        ways = []
        for dz, f in far_first:
            to = dp_to(dz, f)
            copy = remote(zsend.at[b, to], zrecv.at[b, dz, core], peer(tp, to))
            at = counter[0] - 1
            arrives = pltpu.make_async_remote_copy(
                src_ref=zsend.at[b, to],
                dst_ref=zrecv.at[b, dz, other if f else core],
                send_sem=send_sem.at[at],
                recv_sem=recv_sem.at[at],
                device_id=peer(tp, to),
                device_id_type=pl.DeviceIdType.MESH,
            )
            ways.append((dz, to, at, copy, arrives))
        for p in range(3):
            own = jnp.dot(gained, wv[b, 3 * core + p], preferred_element_type=F32)
            pairs[p].wait_recv()
            for j in range(n_dp):
                zsend[b, j, :, p * chans : (p + 1) * chans] = (
                    own[j * PAD : j * PAD + rows]
                    + drecv[b, j, :, p * chans : (p + 1) * chans].astype(F32)
                ).astype(BF16)
                if p == 2:
                    given = drecv[b, j, :, half : half + EXTRA].astype(F32)
                    both = squares[j * PAD : j * PAD + rows] + jnp.sum(
                        given, axis=1, keepdims=True
                    ) * (2.0 / EXTRA)
                    both_high = both.astype(BF16).astype(F32)
                    zsend[b, j, :, half : half + EXTRA] = jnp.where(
                        extra_at < EXTRA // 2, both_high, both - both_high
                    ).astype(BF16)
            for dz, to, at, copy, arrives in ways:
                pltpu.make_async_remote_copy(
                    src_ref=zsend.at[b, to, :, piece[p]],
                    dst_ref=zrecv.at[b, dz, core, :, piece[p]],
                    send_sem=send_sem.at[at],
                    recv_sem=recv_sem.at[at],
                    device_id=peer(tp, to),
                    device_id_type=pl.DeviceIdType.MESH,
                ).start()
        scattered = [(copy, arrives) for dz, to, at, copy, arrives in ways]
        zrecv[b, 0, core] = zsend[b, dp]
        loads[("m", b)].wait()
        for s in range(seqs):
            state = mem[b, s].reshape(heads * size, size)
            state_high = state.astype(BF16)
            s_high[s] = state_high
            s_low[s] = (state - state_high.astype(F32)).astype(BF16)
        fade_b = slot_major(fade_ref[b])
        for copy, arrives in reversed(scattered):
            arrives.wait_recv()
            outgoing.append(copy)

        total_squares = jnp.zeros((rows, 1), F32)
        for dz in range(nz):
            total_squares = total_squares + jnp.sum(
                zrecv[b, dz, 0, :, half : half + EXTRA].astype(F32), axis=1, keepdims=True
            ) * (2.0 / EXTRA)
        row_scale = lax.rsqrt(total_squares / (feats * n_dp) + NORM_EPS)
        for h in range(2):
            total = zrecv[b, 0, h, :, 0:half].astype(F32)
            for dz in range(1, nz):
                total = total + zrecv[b, dz, h, :, 0:half].astype(F32)
            pr[0:rows, h * half : (h + 1) * half] = total * row_scale

        def by_head(p):
            values = pr[:, p * chans : (p + 1) * chans]
            return jnp.stack([values[:, h * size : (h + 1) * size] for h in range(heads)])

        read3, key3, value3 = by_head(0), by_head(1), by_head(2)
        fade3, rate3 = by_head(3), by_head(4)
        ceiling = ceiling_ref[b : b + 1, :]
        decay3 = []
        for h in range(heads):
            extra = jnp.concatenate(
                [fade_b[:, h : h + 1], jnp.zeros((PAD - rows, 1), F32)], axis=0
            )
            decay3.append(
                jnp.exp(
                    extra - ceiling[:, h * size : (h + 1) * size] * jax.nn.sigmoid(fade3[h])
                )
            )
        decay3 = jnp.stack(decay3)
        unit3 = key3 * lax.rsqrt(jnp.sum(key3 * key3, axis=2, keepdims=True) + KEY_EPS)
        pull3 = unit3 * jax.nn.sigmoid(rate3)

        def slots(values):
            return [values[:, t * seqs : (t + 1) * seqs, :] for t in range(steps)]

        read, key, value = slots(read3), slots(key3), slots(value3)
        decay, unit, pull = slots(decay3), slots(unit3), slots(pull3)

        wanted = []
        before = None
        for t in range(steps):
            wanted.append(unit[t] if before is None else before * unit[t])
            before = decay[t] if before is None else before * decay[t]
            wanted.append(before * read[t])
        kinds = len(wanted) * seqs
        deep = -(-kinds // 16) * 16
        wanted = jnp.concatenate(
            wanted + [jnp.zeros((heads, deep - kinds, size), F32)] * (deep > kinds), axis=1
        )
        wanted_high = wanted.astype(BF16).astype(F32)
        wanted_low = wanted - wanted_high
        together = max(d for d in range(1, heads + 1) if heads % d == 0 and d * size <= 256)
        found3 = []
        for first_head in range(0, heads, together):
            span = slice(first_head, first_head + together)
            lhs_high = wanted_high[span].reshape(together * deep, size).astype(BF16)
            lhs_low = wanted_low[span].reshape(together * deep, size).astype(BF16)
            found = None
            kind_at = lax.broadcasted_iota(jnp.int32, (together * deep, 1), 0) % deep % seqs
            for s in range(seqs):
                high_part = s_high[s, first_head * size : (first_head + together) * size, :]
                low_part = s_low[s, first_head * size : (first_head + together) * size, :]
                dims = (((1,), (1,)), ((), ()))
                product = (
                    lax.dot_general(lhs_high, high_part, dims, preferred_element_type=F32)
                    + lax.dot_general(lhs_low, high_part, dims, preferred_element_type=F32)
                    + lax.dot_general(lhs_high, low_part, dims, preferred_element_type=F32)
                )
                found = product if found is None else jnp.where(kind_at == s, product, found)
            for h in range(together):
                found3.append(found[h * deep : (h + 1) * deep, h * size : (h + 1) * size])
        found3 = jnp.stack(found3)
        base = [found3[:, i * seqs : (i + 1) * seqs, :] for i in range(2 * steps)]

        def dot3(a, c):
            return jnp.sum(a * c, axis=2, keepdims=True)

        taken = []

        def state_times(count, start, vector):
            total = start
            for i in range(count - 1, -1, -1):
                total = total - dot3(pull[i], vector) * taken[i] + dot3(key[i], vector) * value[i]
                if i:
                    vector = decay[i] * vector
            return total

        readouts = []
        for t in range(steps):
            taken.append(state_times(t, base[2 * t], unit[t]))
            readouts.append(state_times(t + 1, base[2 * t + 1], read[t]))
        readout = jnp.concatenate(readouts, axis=1)
        centered = readout - jnp.mean(readout, axis=2, keepdims=True)
        normed = centered * lax.rsqrt(
            jnp.mean(centered * centered, axis=2, keepdims=True) + GROUP_EPS
        )
        normed_rows = jnp.concatenate([normed[h] for h in range(heads)], axis=1)
        gate = jax.nn.sigmoid(pr[0:rows, 5 * chans : 6 * chans])
        mixed = normed_rows * rescale_ref[b : b + 1, :] * gate * live_col[0:rows]
        mbuf[b, dp] = mixed.astype(BF16)
        gathered = []
        for dz, f in far_first:
            to = dp_to(dz, f)
            copy = remote(mbuf.at[b, dp], mbuf.at[b, dp], peer(tp, to))
            copy.start()
            gathered.append(copy)

        left, right = [], []
        after = None
        for t in range(steps - 1, -1, -1):
            left += [-taken[t] * live3[t], value[t] * live3[t]]
            right += [pull[t] if after is None else pull[t] * after]
            right += [key[t] if after is None else key[t] * after]
            kept = jnp.where(live3[t] > 0.0, decay[t], 1.0)
            after = kept if after is None else after * kept
        filler = [jnp.zeros((heads, deep - kinds, size), F32)] * (deep > kinds)
        left = jnp.concatenate(left + filler, axis=1)
        right = jnp.concatenate(right + filler, axis=1)
        left_high = left.astype(BF16).astype(F32)
        right_high = right.astype(BF16).astype(F32)
        left = jnp.concatenate([left_high, left - left_high, left_high], axis=1).astype(BF16)
        right = jnp.concatenate([right_high, right_high, right - right_high], axis=1)
        slot_at = lax.broadcasted_iota(jnp.int32, (3 * deep, 1), 0) % deep % seqs
        for s in range(seqs):
            for h in range(heads):
                own = jnp.where(slot_at == s, right[h], 0.0).astype(BF16)
                mem[b, s, h] = mem[b, s, h] * after[h, s : s + 1, :] + lax.dot_general(
                    left[h], own, (((0,), (0,)), ((), ())), preferred_element_type=F32
                )
        store = pltpu.make_async_copy(mem.at[b], state_hbm.at[b], store_sem.at[b])
        store.start()
        loads[("s", b)] = store
        for copy in reversed(gathered):
            copy.wait_recv()
        outgoing += gathered
        for j in range(n_dp):
            ms[j * PAD : j * PAD + rows, :] = mbuf[b, j].astype(F32)
        loads[("e", b)].wait()
        part = jnp.dot(ms[...].astype(BF16), ev[b], preferred_element_type=F32)
        for j in range(n_dp):
            psend[b, j] = part[j * PAD : j * PAD + rows].astype(BF16)
        if b < blocks - 1:
            shared = []
            for k in range(1, n_tp):
                copy = remote(psend.at[b], precv.at[b, k - 1], peer(tp_to(k), dp))
                copy.start()
                shared.append(copy)
            for copy in shared:
                copy.wait_recv()
            outgoing += shared
            for j in range(n_dp):
                at = j * PAD
                total = part[at : at + rows]
                for k in range(1, n_tp):
                    total = total + precv[b, k - 1, j].astype(F32)
                xs[at : at + rows, :] = (x_now[at : at + rows] + total).astype(BF16).astype(F32)
        else:
            pown[:, 0:feats] = part
            shared = []
            for k in range(1, n_tp):
                copy = remote(
                    psend.at[b, pl.ds(tp_to(k) * per_tp, per_tp)],
                    precv.at[b, k - 1, pl.ds(0, per_tp)],
                    peer(tp_to(k), dp),
                )
                copy.start()
                shared.append(copy)
            for copy in shared:
                copy.wait_recv()
            outgoing += shared
            pieces = []
            for g in range(per_tp):
                at = pl.multiple_of((tp * per_tp + g) * PAD, PAD)
                total = pown[pl.ds(at, PAD), 0:feats][0:rows]
                for k in range(1, n_tp):
                    total = total + precv[b, k - 1, g].astype(F32)
                pieces.append(sequence_major(xs[pl.ds(at, PAD), :][0:rows] + total))
            out_ref[...] = jnp.concatenate(pieces, axis=0).astype(BF16)

    for b in range(blocks):
        loads[("s", b)].wait()
    for copy in outgoing:
        copy.wait_send()


def solution(mesh):
    n_tp, n_dp = mesh.shape["tp"], mesh.shape["dp"]

    def shards(
        hidden,
        live,
        gain,
        w0,
        w1,
        w2,
        w3,
        w4,
        w5,
        ceiling,
        rescale,
        exit_w,
        memories,
        fade,
    ):
        blocks, feats, chans = w0.shape
        seqs, heads, size = memories.shape[1], memories.shape[2], memories.shape[3]
        rows = fade.shape[1]
        nz = n_dp // 2
        width = 3 * chans + EXTRA
        copies = (n_tp - 1) * (1 + blocks) + blocks * (3 + 2 * (n_dp - 1))
        vmem = pl.BlockSpec(memory_space=pltpu.VMEM)
        smem = pl.BlockSpec(memory_space=pltpu.SMEM)
        hbm = pl.BlockSpec(memory_space=pl.ANY)
        return pl.pallas_call(
            functools.partial(kernel, n_tp, n_dp),
            out_shape=(
                jax.ShapeDtypeStruct(hidden.shape, hidden.dtype),
                jax.ShapeDtypeStruct(memories.shape, memories.dtype),
            ),
            in_specs=[hbm, smem] + [hbm] * 12,
            out_specs=(vmem, hbm),
            scratch_shapes=[
                pltpu.VMEM((blocks, 6, feats, chans), BF16),
                pltpu.VMEM((blocks, chans, feats), BF16),
                pltpu.VMEM((blocks, seqs, heads, size, size), F32),
                pltpu.VMEM((n_tp,) + hidden.shape, BF16),
                pltpu.VMEM((n_dp * PAD, feats), F32),
                pltpu.VMEM((n_dp * PAD, chans), F32),
                pltpu.VMEM((n_dp * PAD, 3 * chans), F32),
                pltpu.VMEM((blocks, n_dp, rows, width), BF16),
                pltpu.VMEM((blocks, n_dp, rows, width), BF16),
                pltpu.VMEM((blocks, n_dp, rows, width), BF16),
                pltpu.VMEM((blocks, nz, 2, rows, width), BF16),
                pltpu.VMEM((PAD, 6 * chans), F32),
                pltpu.VMEM((blocks, n_dp, rows, chans), BF16),
                pltpu.VMEM((blocks, n_dp, rows, feats), BF16),
                pltpu.VMEM((blocks, n_tp - 1, n_dp, rows, feats), BF16),
                pltpu.VMEM(gain.shape, BF16),
                pltpu.VMEM(ceiling.shape, F32),
                pltpu.VMEM(rescale.shape, F32),
                pltpu.VMEM(fade.shape, F32),
                pltpu.VMEM((seqs, heads * size, size), BF16),
                pltpu.VMEM((seqs, heads * size, size), BF16),
                pltpu.SemaphoreType.DMA((blocks * 8 + 5,)),
                pltpu.SemaphoreType.DMA((blocks,)),
                pltpu.SemaphoreType.DMA((copies,)),
                pltpu.SemaphoreType.DMA((copies,)),
            ],
            compiler_params=pltpu.CompilerParams(
                collective_id=0, has_side_effects=True, vmem_limit_bytes=67043328
            ),
        )(hidden, live, gain, w0, w1, w2, w3, w4, w5, ceiling, rescale, exit_w, memories, fade)

    in_specs = (
        P("tp", "dp"),
        P("dp"),
        P(None, "dp"),
        P(None, "dp", "tp"),
        P(None, "dp", "tp"),
        P(None, "dp", "tp"),
        P(None, "dp", "tp"),
        P(None, "dp", "tp"),
        P(None, "dp", "tp"),
        P(None, "tp"),
        P(None, "tp"),
        P(None, "tp", "dp"),
        P(None, "dp", "tp", None, None),
        P(None, "dp", "tp"),
    )
    out_specs = (P("tp", "dp"), P(None, "dp", "tp", None, None))
    return jax.shard_map(shards, mesh=mesh, in_specs=in_specs, out_specs=out_specs, check_vma=False)
```

profile of v0, /device:TPU:0, one launch (start us, length us, event | category | flops | bytes accessed | tf_op | source)
XLA Modules:
  0.0 52.0 jit_solution(7626347553666172460)
XLA Ops:
  0.6 1.3 %copy.16.fade_hbm = f32[2,6,8]{2,1,0:T(8,128)} copy(f32[2,6,8]{2,0,1:T(2,128)} %param.27) | data formatting | bytes 768 | tf_op args[13]
  1.9 46.0 %shard_map.149 = (bf16[12,512]{1,0:T(8,128)(2,1)}, f32[2,3,8,64,64]{4,3,2,1,0:T(8,128)}) custom-call(bf16[12,512]{1,0:T(8,128)(2,1)} %x_hbm.1, s32[3]{0:T(128)} %live_ref.1, bf16[2,512]{1,0:T(2,128)(2,1)} %gain_hbm.1, bf16[2,512,512]{2,1,0:T(8,128)(2,1)} %w0.1, bf16[2,512,512]{2,1,0:T(8,128)(2,1)} %w1.1, bf16[2,512,512]{2,1,0:T(8,128)(2,1)} %w2.1, ...), custom_call_target="tpu_custom_call" | custom-call | tf_op jit(solution)/shard_map/pallas_call | solution.py:487
  47.9 1.3 %copy.19 = bf16[12,512]{1,0:T(8,128)(2,1)} copy(bf16[12,512]{1,0:T(8,128)(2,1)} %get-tuple-element.4) | data formatting | bytes 24576
  49.2 2.7 %copy.20 = f32[2,3,8,64,64]{4,3,2,1,0:T(8,128)} copy(f32[2,3,8,64,64]{4,3,2,1,0:T(8,128)} %get-tuple-element.5) | data formatting | bytes 1572864
where the time goes:
time: 52.4 us; the launch traced here: 52 us
  Pallas kernels  46 us (88%)
  local copies, waits for them, and re-layouts  5.34 us (10%)
  between operations  0.64 us (1%)
    pallas_call x1, Pallas kernels, shards(): pl.pallas_call(functools.partial(kernel, n_tp, n_dp), out_shape=(jax.Shap...  46 us
    unnamed x3, local copies, waits for them, and re-layouts  5.34 us

commit v1 on v0

--- a/solution.py
+++ b/solution.py
@@ -265,7 +265,7 @@
             state_high = state.astype(BF16)
             s_high[s] = state_high
             s_low[s] = (state - state_high.astype(F32)).astype(BF16)
-        fade_b = slot_major(fade_ref[b])
+        fade_b = slot_major(fade_ref[:, b, :])
         for copy, arrives in reversed(scattered):
             arrives.wait_recv()
             outgoing.append(copy)
@@ -397,12 +397,9 @@
         for s in range(seqs):
             for h in range(heads):
                 own = jnp.where(slot_at == s, right[h], 0.0).astype(BF16)
-                mem[b, s, h] = mem[b, s, h] * after[h, s : s + 1, :] + lax.dot_general(
+                state_hbm[b, s, h] = mem[b, s, h] * after[h, s : s + 1, :] + lax.dot_general(
                     left[h], own, (((0,), (0,)), ((), ())), preferred_element_type=F32
                 )
-        store = pltpu.make_async_copy(mem.at[b], state_hbm.at[b], store_sem.at[b])
-        store.start()
-        loads[("s", b)] = store
         for copy in reversed(gathered):
             copy.wait_recv()
         outgoing += gathered
@@ -450,10 +447,19 @@
                 pieces.append(sequence_major(xs[pl.ds(at, PAD), :][0:rows] + total))
             out_ref[...] = jnp.concatenate(pieces, axis=0).astype(BF16)
 
-    for b in range(blocks):
-        loads[("s", b)].wait()
     for copy in outgoing:
         copy.wait_send()
+
+
+def store_kernel(out_vmem, state_vmem, out_hbm, state_hbm, sem):
+    copies = [
+        pltpu.make_async_copy(state_vmem, state_hbm, sem.at[0]),
+        pltpu.make_async_copy(out_vmem, out_hbm, sem.at[1]),
+    ]
+    for copy in copies:
+        copy.start()
+    for copy in copies:
+        copy.wait()
 
 
 def solution(mesh):
@@ -483,15 +489,15 @@
         copies = (n_tp - 1) * (1 + blocks) + blocks * (3 + 2 * (n_dp - 1))
         vmem = pl.BlockSpec(memory_space=pltpu.VMEM)
         smem = pl.BlockSpec(memory_space=pltpu.SMEM)
-        hbm = pl.BlockSpec(memory_space=pl.ANY)
-        return pl.pallas_call(
+        hbm = pl.BlockSpec(memory_space=pltpu.HBM)
+        placed = pl.pallas_call(
             functools.partial(kernel, n_tp, n_dp),
             out_shape=(
-                jax.ShapeDtypeStruct(hidden.shape, hidden.dtype),
-                jax.ShapeDtypeStruct(memories.shape, memories.dtype),
+                pltpu.VMEM(hidden.shape, hidden.dtype),
+                pltpu.VMEM(memories.shape, memories.dtype),
             ),
             in_specs=[hbm, smem] + [hbm] * 12,
-            out_specs=(vmem, hbm),
+            out_specs=(vmem, vmem),
             scratch_shapes=[
                 pltpu.VMEM((blocks, 6, feats, chans), BF16),
                 pltpu.VMEM((blocks, chans, feats), BF16),
@@ -511,7 +517,7 @@
                 pltpu.VMEM(gain.shape, BF16),
                 pltpu.VMEM(ceiling.shape, F32),
                 pltpu.VMEM(rescale.shape, F32),
-                pltpu.VMEM(fade.shape, F32),
+                pltpu.VMEM((rows, blocks, fade.shape[2]), F32),
                 pltpu.VMEM((seqs, heads * size, size), BF16),
                 pltpu.VMEM((seqs, heads * size, size), BF16),
                 pltpu.SemaphoreType.DMA((blocks * 8 + 5,)),
@@ -520,9 +526,20 @@
                 pltpu.SemaphoreType.DMA((copies,)),
             ],
             compiler_params=pltpu.CompilerParams(
-                collective_id=0, has_side_effects=True, vmem_limit_bytes=67043328
+                collective_id=0, has_side_effects=True, vmem_limit_bytes=50000000
             ),
-        )(hidden, live, gain, w0, w1, w2, w3, w4, w5, ceiling, rescale, exit_w, memories, fade)
+        )(hidden, live, gain, w0, w1, w2, w3, w4, w5, ceiling, rescale, exit_w, memories, fade.transpose(1, 0, 2))
+        return pl.pallas_call(
+            store_kernel,
+            out_shape=(
+                jax.ShapeDtypeStruct(hidden.shape, hidden.dtype),
+                jax.ShapeDtypeStruct(memories.shape, memories.dtype),
+            ),
+            in_specs=[vmem, vmem],
+            out_specs=(hbm, hbm),
+            scratch_shapes=[pltpu.SemaphoreType.DMA((2,))],
+            compiler_params=pltpu.CompilerParams(vmem_limit_bytes=1048576),
+        )(*placed)
 
     in_specs = (
         P("tp", "dp"),

time: 52.4 us -> 56.9 us (1.086)
  local copies, waits for them, and re-layouts: 5.34 us -> 9.01 us
  Pallas kernels: 46 us -> 46.7 us
    unnamed x3 -> x20, local copies, waits for them, and re-layouts: 5.34 us -> 9.01 us
    pallas_call x1 -> x2, Pallas kernels: 46 us -> 46.7 us  [the longest x1 45.6 us: shards(): pl.pallas_call(functools.partial(kernel, n_tp, n_dp), out_shape=(pltpu.VM...]
where the time goes in v1:
time: 56.9 us; the launch traced here: 56.4 us
  Pallas kernels  46.7 us (82%)
  local copies, waits for them, and re-layouts  9.01 us (16%)
  between operations  0.66 us (1%)
    pallas_call x1, Pallas kernels, shards(): pl.pallas_call(functools.partial(kernel, n_tp, n_dp), out_shape=(pltpu.VM...  45.6 us
    unnamed x20, local copies, waits for them, and re-layouts  9.01 us
    pallas_call x1, Pallas kernels, shards(): pl.pallas_call(store_kernel, out_shape=(jax.ShapeDtypeStruct(hidden.shape...  1.16 us

profile of v1, /device:TPU:0, one launch (start us, length us, event | category | flops | bytes accessed | tf_op | source)
XLA Modules:
  0.0 56.4 jit_solution(756746777698491018)
XLA Ops:
  0.6 0.0 copy-start
  0.6 1.2 %copy-done = bf16[2,512,512]{2,1,0:T(8,128)(2,1)S(1)} copy-done((bf16[2,512,512]{2,1,0:T(8,128)(2,1)S(1)}, bf16[2,512,512]{2,1,0:T(8,128)(2,1)}, u32[]{:S(2)}) %copy-start) | copy-done | bytes 1048600
  1.9 0.0 copy-start.1
  1.9 1.2 %copy-done.1 = bf16[2,512,512]{2,1,0:T(8,128)(2,1)S(1)} copy-done((bf16[2,512,512]{2,1,0:T(8,128)(2,1)S(1)}, bf16[2,512,512]{2,1,0:T(8,128)(2,1)}, u32[]{:S(2)}) %copy-start.1) | copy-done | bytes 1048600
  3.1 0.0 copy-start.2
  3.1 1.2 %copy-done.2 = bf16[2,512,512]{2,1,0:T(8,128)(2,1)S(1)} copy-done((bf16[2,512,512]{2,1,0:T(8,128)(2,1)S(1)}, bf16[2,512,512]{2,1,0:T(8,128)(2,1)}, u32[]{:S(2)}) %copy-start.2) | copy-done | bytes 1048600
  4.3 0.0 copy-start.3
  4.3 1.2 %copy-done.3 = bf16[2,512,512]{2,1,0:T(8,128)(2,1)S(1)} copy-done((bf16[2,512,512]{2,1,0:T(8,128)(2,1)S(1)}, bf16[2,512,512]{2,1,0:T(8,128)(2,1)}, u32[]{:S(2)}) %copy-start.3) | copy-done | bytes 1048600
  5.5 0.0 copy-start.4
  5.5 0.7 %copy-done.4 = bf16[12,512]{1,0:T(8,128)(2,1)S(1)} copy-done((bf16[12,512]{1,0:T(8,128)(2,1)S(1)}, bf16[12,512]{1,0:T(8,128)(2,1)}, u32[]{:S(2)}) %copy-start.4) | copy-done | bytes 12312
  6.3 0.0 copy-start.5
  6.3 0.7 %copy-done.5 = f32[2,6,8]{2,0,1:T(2,128)S(1)} copy-done((f32[2,6,8]{2,0,1:T(2,128)S(1)}, f32[2,6,8]{2,0,1:T(2,128)}, u32[]{:S(2)}) %copy-start.5) | copy-done | bytes 408
  6.9 0.0 copy-start.6
  6.9 0.7 %copy-done.6 = f32[2,512]{1,0:T(2,128)S(1)} copy-done((f32[2,512]{1,0:T(2,128)S(1)}, f32[2,512]{1,0:T(2,128)}, u32[]{:S(2)}) %copy-start.6) | copy-done | bytes 4120
  7.6 0.0 copy-start.7
  7.6 0.7 %copy-done.7 = f32[2,512]{1,0:T(2,128)S(1)} copy-done((f32[2,512]{1,0:T(2,128)S(1)}, f32[2,512]{1,0:T(2,128)}, u32[]{:S(2)}) %copy-start.7) | copy-done | bytes 4120
  8.3 0.0 copy-start.8
  8.3 0.7 %copy-done.8 = bf16[2,512]{1,0:T(2,128)(2,1)S(1)} copy-done((bf16[2,512]{1,0:T(2,128)(2,1)S(1)}, bf16[2,512]{1,0:T(2,128)(2,1)}, u32[]{:S(2)}) %copy-start.8) | copy-done | bytes 2072
  9.0 0.0 copy-start.9
  9.0 0.7 %copy-done.9 = s32[3]{0:T(128)S(1)} copy-done((s32[3]{0:T(128)S(1)}, s32[3]{0:T(128)}, u32[]{:S(2)}) %copy-start.9) | copy-done | bytes 36
  9.7 45.6 %shard_map.149 = (bf16[12,512]{1,0:T(8,128)(2,1)S(1)}, f32[2,3,8,64,64]{4,3,2,1,0:T(8,128)S(1)}) custom-call(bf16[12,512]{1,0:T(8,128)(2,1)S(1)} %copy-done.4, s32[3]{0:T(128)S(1)} %copy-done.9, bf16[2,512]{1,0:T(2,128)(2,1)S(1)} %copy-done.8, bf16[2,512,512]{2,1,0:T(8,128)(2,1)S(1)} %copy-done, bf16[2,512,512]{2,1,0:T(8,128)(2,1)S(1)} %copy-done.1, ...), custom_call_target="tpu_custom_call" | custom-call | tf_op jit(solution)/shard_map/pallas_call | solution.py:493
  55.2 1.2 %shard_map.150 = (bf16[12,512]{1,0:T(8,128)(2,1)}, f32[2,3,8,64,64]{4,3,2,1,0:T(8,128)}) custom-call(bf16[12,512]{1,0:T(8,128)(2,1)S(1)} %get-tuple-element.4.out_vmem, f32[2,3,8,64,64]{4,3,2,1,0:T(8,128)S(1)} %get-tuple-element.5.state_vmem), custom_call_target="tpu_custom_call" | custom-call | tf_op jit(solution)/shard_map/pallas_call | solution.py:532
Async XLA Ops:
  0.6 1.2 %copy-start = (bf16[2,512,512]{2,1,0:T(8,128)(2,1)S(1)}, bf16[2,512,512]{2,1,0:T(8,128)(2,1)}, u32[]{:S(2)}) copy-start(bf16[2,512,512]{2,1,0:T(8,128)(2,1)} %w0.1) | copy-start | bytes 3145732
  1.9 1.2 %copy-start.1 = (bf16[2,512,512]{2,1,0:T(8,128)(2,1)S(1)}, bf16[2,512,512]{2,1,0:T(8,128)(2,1)}, u32[]{:S(2)}) copy-start(bf16[2,512,512]{2,1,0:T(8,128)(2,1)} %w1.1) | copy-start | bytes 3145732
  3.1 1.2 %copy-start.2 = (bf16[2,512,512]{2,1,0:T(8,128)(2,1)S(1)}, bf16[2,512,512]{2,1,0:T(8,128)(2,1)}, u32[]{:S(2)}) copy-start(bf16[2,512,512]{2,1,0:T(8,128)(2,1)} %w2.1) | copy-start | bytes 3145732
  4.3 1.2 %copy-start.3 = (bf16[2,512,512]{2,1,0:T(8,128)(2,1)S(1)}, bf16[2,512,512]{2,1,0:T(8,128)(2,1)}, u32[]{:S(2)}) copy-start(bf16[2,512,512]{2,1,0:T(8,128)(2,1)} %w3.1) | copy-start | bytes 3145732
  5.5 0.7 %copy-start.4 = (bf16[12,512]{1,0:T(8,128)(2,1)S(1)}, bf16[12,512]{1,0:T(8,128)(2,1)}, u32[]{:S(2)}) copy-start(bf16[12,512]{1,0:T(8,128)(2,1)} %x_hbm.1) | copy-start | bytes 36868
  6.3 0.7 %copy-start.5 = (f32[2,6,8]{2,0,1:T(2,128)S(1)}, f32[2,6,8]{2,0,1:T(2,128)}, u32[]{:S(2)}) copy-start(f32[2,6,8]{2,0,1:T(2,128)} %param.27) | copy-start | bytes 1156
  6.9 0.7 %copy-start.6 = (f32[2,512]{1,0:T(2,128)S(1)}, f32[2,512]{1,0:T(2,128)}, u32[]{:S(2)}) copy-start(f32[2,512]{1,0:T(2,128)} %ceiling_hbm.1) | copy-start | bytes 12292
  7.6 0.7 %copy-start.7 = (f32[2,512]{1,0:T(2,128)S(1)}, f32[2,512]{1,0:T(2,128)}, u32[]{:S(2)}) copy-start(f32[2,512]{1,0:T(2,128)} %rescale_hbm.1) | copy-start | bytes 12292
  8.3 0.7 %copy-start.8 = (bf16[2,512]{1,0:T(2,128)(2,1)S(1)}, bf16[2,512]{1,0:T(2,128)(2,1)}, u32[]{:S(2)}) copy-start(bf16[2,512]{1,0:T(2,128)(2,1)} %gain_hbm.1) | copy-start | bytes 6148
  9.0 0.7 %copy-start.9 = (s32[3]{0:T(128)S(1)}, s32[3]{0:T(128)}, u32[]{:S(2)}) copy-start(s32[3]{0:T(128)} %live_ref.1) | copy-start | bytes 40

commit v2 on v1

--- a/solution.py
+++ b/solution.py
@@ -11,6 +11,8 @@
 KEY_EPS = 1e-06
 GROUP_EPS = 0.00064
 PAD = 8
+LANES = 128
+VMEM_BYTES = 67043328
 EXTRA = 128
 F32 = jnp.float32
 BF16 = jnp.bfloat16
@@ -487,9 +489,11 @@
         nz = n_dp // 2
         width = 3 * chans + EXTRA
         copies = (n_tp - 1) * (1 + blocks) + blocks * (3 + 2 * (n_dp - 1))
+        outputs = 4 * blocks * seqs * heads * size * (-(-size // LANES) * LANES)
+        outputs += 4 * hidden.shape[0] * hidden.shape[1]
         vmem = pl.BlockSpec(memory_space=pltpu.VMEM)
         smem = pl.BlockSpec(memory_space=pltpu.SMEM)
-        hbm = pl.BlockSpec(memory_space=pltpu.HBM)
+        hbm = pl.BlockSpec(memory_space=pl.ANY)
         placed = pl.pallas_call(
             functools.partial(kernel, n_tp, n_dp),
             out_shape=(
@@ -526,7 +530,7 @@
                 pltpu.SemaphoreType.DMA((copies,)),
             ],
             compiler_params=pltpu.CompilerParams(
-                collective_id=0, has_side_effects=True, vmem_limit_bytes=50000000
+                collective_id=0, has_side_effects=True, vmem_limit_bytes=VMEM_BYTES - outputs
             ),
         )(hidden, live, gain, w0, w1, w2, w3, w4, w5, ceiling, rescale, exit_w, memories, fade.transpose(1, 0, 2))
         return pl.pallas_call(

time: 56.9 us -> 47.5 us (0.83)
  local copies, waits for them, and re-layouts: 9.01 us -> 0 us
    unnamed x20 -> x0, local copies, waits for them, and re-layouts: 9.01 us -> none
where the time goes in v2:
time: 47.5 us; the launch traced here: 47.2 us
  Pallas kernels  46.6 us (98%)
  between operations  0.64 us (1%)
    pallas_call x1, Pallas kernels, shards(): pl.pallas_call(functools.partial(kernel, n_tp, n_dp), out_shape=(pltpu.VM...  45.4 us
    pallas_call x1, Pallas kernels, shards(): pl.pallas_call(store_kernel, out_shape=(jax.ShapeDtypeStruct(hidden.shape...  1.16 us

profile of v2, /device:TPU:0, one launch (start us, length us, event | category | flops | bytes accessed | tf_op | source)
XLA Modules:
  0.0 47.2 jit_solution(9801535325212853553)
XLA Ops:
  0.6 45.4 %shard_map.149 = (bf16[12,512]{1,0:T(8,128)(2,1)S(1)}, f32[2,3,8,64,64]{4,3,2,1,0:T(8,128)S(1)}) custom-call(bf16[12,512]{1,0:T(8,128)(2,1)} %x_hbm.1, s32[3]{0:T(128)} %live_ref.1, bf16[2,512]{1,0:T(2,128)(2,1)} %gain_hbm.1, bf16[2,512,512]{2,1,0:T(8,128)(2,1)} %w0.1, bf16[2,512,512]{2,1,0:T(8,128)(2,1)} %w1.1, bf16[2,512,512]{2,1,0:T(8,128)(2,1)} %w2.1, ...), custom_call_target="tpu_custom_call" | custom-call | tf_op jit(solution)/shard_map/pallas_call | solution.py:497
  46.1 1.2 %shard_map.150 = (bf16[12,512]{1,0:T(8,128)(2,1)}, f32[2,3,8,64,64]{4,3,2,1,0:T(8,128)}) custom-call(bf16[12,512]{1,0:T(8,128)(2,1)S(1)} %get-tuple-element.4.out_vmem, f32[2,3,8,64,64]{4,3,2,1,0:T(8,128)S(1)} %get-tuple-element.5.state_vmem), custom_call_target="tpu_custom_call" | custom-call | tf_op jit(solution)/shard_map/pallas_call | solution.py:536

commit v3 on v2

v3 whole, which is shorter than its diff:
```python
import functools

import jax
import jax.numpy as jnp
from jax import lax
from jax.experimental import pallas as pl
from jax.experimental.pallas import tpu as pltpu
from jax.sharding import PartitionSpec as P

NORM_EPS = 1e-06
KEY_EPS = 1e-06
GROUP_EPS = 0.00064
PAD = 8
LANES = 128
WIDEST = 256
VMEM_BYTES = 67043328
F32 = jnp.float32
BF16 = jnp.bfloat16


def packing(tiles, rows, extra):
    spare = PAD - rows
    kept = next(k for k in range(1, tiles + 2) if k * spare >= max(tiles - k, 0) * rows + extra)
    kept = max(kept, 1)
    stream = [(u, r) for u in range(kept, tiles) for r in range(rows)]
    stream += [(None, r) for r in range(extra)]
    return kept, [stream[t * spare : (t + 1) * spare] for t in range(kept)]


def runs(slots):
    found = []
    for at, (u, r) in enumerate(slots):
        if found and found[-1][0] == u and found[-1][2] == r:
            found[-1][2] = r + 1
        else:
            found.append([u, r, r + 1, at])
    return found


def pack(tiles, rows, extra):
    kept, slots = packing(len(tiles), rows, len(extra))
    packed = []
    for t in range(kept):
        parts = [tiles[t][0:rows] if t < len(tiles) else jnp.zeros((rows, LANES), F32)]
        for u, first, last, at in runs(slots[t]):
            parts += extra[first:last] if u is None else [tiles[u][first:last]]
        missing = PAD - rows - len(slots[t])
        if missing:
            parts.append(jnp.zeros((missing, LANES), F32))
        packed.append(jnp.concatenate(parts, axis=0))
    return jnp.concatenate(packed, axis=1)


def unpack(packed, tiles, rows, extra):
    kept, slots = packing(tiles, rows, extra)
    cut = [packed[:, t * LANES : (t + 1) * LANES] for t in range(kept)]
    moved, found = {}, []
    for t in range(kept):
        for u, first, last, at in runs(slots[t]):
            piece = cut[t][rows + at : rows + at + last - first]
            if u is None:
                found += [piece[i : i + 1] for i in range(last - first)]
            else:
                moved.setdefault(u, []).append(piece)
    for u in range(kept, tiles):
        parts = moved[u] + [jnp.zeros((PAD - rows, LANES), F32)]
        cut.append(jnp.concatenate(parts, axis=0))
    return jnp.concatenate(cut[:tiles], axis=1), found


def pieces_of(groups):
    pieces = []
    for g in range(groups):
        pieces += [(g, True, (0,)), (g, False, (1, 2))] if g == 0 else [
            (g, False, (0, 1)),
            (g, False, (2,)),
        ]
    return pieces


def piece_shape(piece, per_proj):
    g, whole, kinds = piece
    return len(kinds) * per_proj * (2 if whole else 1), 2 if whole else 0


def kernel(
    n_tp,
    n_dp,
    x_hbm,
    live_ref,
    gain_hbm,
    w0,
    w1,
    w2,
    w3,
    w4,
    w5,
    ceiling_hbm,
    rescale_hbm,
    exit_hbm,
    memory_hbm,
    fade_hbm,
    out_ref,
    state_ref,
    wv,
    ev,
    mem,
    gx,
    xs,
    pown,
    dsend,
    drecv,
    mbuf,
    psend,
    precv,
    gain_ref,
    ceiling_ref,
    rescale_ref,
    fade_ref,
    s_cat,
    load_sem,
    send_sem,
    recv_sem,
    *piece_refs,
):
    blocks = wv.shape[0]
    feats = x_hbm.shape[1]
    seqs, heads, size = mem.shape[1], mem.shape[2], mem.shape[3]
    rows = fade_hbm.shape[0]
    steps = rows // seqs
    groups, wide = mbuf.shape[1], mbuf.shape[4]
    together = heads // groups
    nz = n_dp // 2
    per_tp = n_dp // n_tp
    per_proj = wide // LANES
    pieces = pieces_of(groups)
    zsend, zrecv = piece_refs[0::2], piece_refs[1::2]
    feat_tiles = feats // LANES

    tp = lax.axis_index("tp")
    dp = lax.axis_index("dp")
    z = dp // 2
    core = dp % 2
    other = 1 - core

    def peer(tp_at, dp_at):
        return {"tp": tp_at, "dp": dp_at}

    def tp_to(m):
        at, bit = tp * 0, 1
        while bit < n_tp:
            mine = (tp // bit) % 2
            at = at + bit * ((1 - mine) if m & bit else mine)
            bit *= 2
        return at

    def dp_to(dz, flip):
        return lax.rem(z + dz, nz) * 2 + (other if flip else core)

    tp_offsets = sorted(range(1, n_tp), key=lambda m: -bin(m).count("1"))
    dp_offsets = [(dz, f) for dz in range(nz) for f in range(2) if (dz, f) != (0, 0)]
    far_first = sorted(dp_offsets, key=lambda o: -min(o[0], nz - o[0]))

    def slot_major(values):
        return jnp.concatenate(
            [
                values[s * steps + t : s * steps + t + 1]
                for t in range(steps)
                for s in range(seqs)
            ],
            axis=0,
        )

    def sequence_major(values):
        return jnp.concatenate(
            [
                values[t * seqs + s : t * seqs + s + 1]
                for s in range(seqs)
                for t in range(steps)
            ],
            axis=0,
        )

    counter = [0]

    def remote(src, dst, to, lands=None):
        at = counter[0]
        counter[0] += 1

        def copy(dst_ref):
            return pltpu.make_async_remote_copy(
                src_ref=src,
                dst_ref=dst_ref,
                send_sem=send_sem.at[at],
                recv_sem=recv_sem.at[at],
                device_id=to,
                device_id_type=pl.DeviceIdType.MESH,
            )

        sent = copy(dst)
        sent.start()
        outgoing.append(sent)
        return sent if lands is None else copy(lands)

    outgoing = []
    weights = (w1, w0, w2, w3, w4, w5)
    loads = {}

    def load(name, src, dst):
        copy = pltpu.make_async_copy(src, dst, load_sem.at[len(loads)])
        copy.start()
        loads[name] = copy

    load("x", x_hbm, gx.at[tp])
    load("gain", gain_hbm, gain_ref)
    load("ceiling", ceiling_hbm, ceiling_ref)
    load("rescale", rescale_hbm, rescale_ref)
    load("fade", fade_hbm, fade_ref)
    for b in range(blocks):
        for p in range(6):
            load(("w", b, p), weights[p].at[b], wv.at[b, p])
        load(("m", b), memory_hbm.at[b], mem.at[b])
        load(("e", b), exit_hbm.at[b], ev.at[b])

    barrier = pltpu.get_barrier_semaphore()
    for m in tp_offsets:
        pl.semaphore_signal(
            barrier, inc=1, device_id=peer(tp_to(m), dp), device_id_type=pl.DeviceIdType.MESH
        )
    for dz, f in far_first:
        pl.semaphore_signal(
            barrier, inc=1, device_id=peer(tp, dp_to(dz, f)), device_id_type=pl.DeviceIdType.MESH
        )
    xs[...] = jnp.zeros_like(xs)
    loads["x"].wait()
    pl.semaphore_wait(barrier, n_tp - 1 + len(dp_offsets))

    first = []
    for m in tp_offsets:
        first.append(remote(gx.at[tp], gx.at[tp], peer(tp_to(m), dp), gx.at[tp_to(m)]))

    row_at = lax.broadcasted_iota(jnp.int32, (PAD, 1), 0)
    live_col = jnp.zeros((PAD, 1), F32)
    for s in range(seqs):
        for t in range(steps):
            live_col = jnp.where(
                row_at == t * seqs + s, jnp.where(live_ref[s] > t, 1.0, 0.0), live_col
            )
    live3 = [
        live_col[t * seqs : (t + 1) * seqs].reshape(1, seqs, 1) for t in range(steps)
    ]
    on_row = lax.broadcasted_iota(jnp.int32, (n_dp * PAD, LANES), 1) == (
        lax.broadcasted_iota(jnp.int32, (n_dp * PAD, LANES), 0) % PAD
    )
    kinds = 2 * steps * seqs
    deep = -(-kinds // 16) * 16
    kind_at = lax.broadcasted_iota(jnp.int32, (together * deep, 1), 0) % deep % seqs
    slot_at = lax.broadcasted_iota(jnp.int32, (3 * deep, 1), 0) % deep % seqs
    filler = [jnp.zeros((together, deep - kinds, size), F32)] * (deep > kinds)

    def split_states(b):
        loads[("m", b)].wait()
        for s in range(seqs):
            state = mem[b, s].reshape(heads * size, size)
            high = state.astype(BF16)
            low = (state - high.astype(F32)).astype(BF16)
            s_cat[b, s, :, 0:size] = high
            s_cat[b, s, :, size : 2 * size] = high
            s_cat[b, s, :, 2 * size : 3 * size] = low

    for name in ("gain", "ceiling", "rescale", "fade"):
        loads[name].wait()
    split_states(0)
    for p in range(6):
        loads[("w", 0, p)].wait()
    for copy in first:
        copy.wait_recv()
    for i in range(n_tp):
        whole = gx[i].astype(F32)
        for g in range(per_tp):
            xs[(i * per_tp + g) * PAD : (i * per_tp + g) * PAD + rows, :] = slot_major(
                whole[g * rows : (g + 1) * rows]
            )

    for b in range(blocks):
        x_now = xs[...]
        gained = (x_now * gain_ref[b : b + 1, :].astype(F32)).astype(BF16)

        def project(slots, g):
            return jnp.concatenate(
                [
                    jnp.dot(
                        gained,
                        wv[b, p, :, g * wide : (g + 1) * wide],
                        preferred_element_type=F32,
                    )
                    for p in slots
                ],
                axis=1,
            )

        scattered = {}

        def scatter(i, values):
            tiles, extra = piece_shape(pieces[i], per_proj)
            for j in range(n_dp):
                block = values[j * PAD : (j + 1) * PAD]
                cut = [block[:, t * LANES : (t + 1) * LANES] for t in range(tiles)]
                noted = [lined_high[j : j + 1], lined_low[j : j + 1]] if extra else []
                zsend[i][b, j] = pack(cut, rows, noted).astype(BF16)
            ways = []
            for dz, f in far_first:
                to = dp_to(dz, f)
                ways.append(
                    remote(
                        zsend[i].at[b, to],
                        zrecv[i].at[b, dz, core],
                        peer(tp, to),
                        zrecv[i].at[b, dz, other if f else core],
                    )
                )
            scattered[i] = ways

        halves = [
            sorted(k for g_at, whole, kinds in pieces if g_at == g and not whole for k in kinds)
            for g in range(groups)
        ]
        pairs, own = [], []

        def give(g):
            width = len(halves[g]) * wide
            dsend[b, g, :, 0:width] = project([3 * other + k for k in halves[g]], g).astype(BF16)
            pairs.append(
                remote(
                    dsend.at[b, g, :, pl.ds(0, width)],
                    drecv.at[b, g, :, pl.ds(0, width)],
                    peer(tp, dp_to(0, 1)),
                )
            )

        give(0)
        squares = jnp.sum(x_now * x_now, axis=1, keepdims=True)
        lined = jnp.where(on_row, squares, 0.0).reshape(n_dp, PAD, LANES)
        lined = jnp.sum(lined, axis=1)
        lined_high = lined.astype(BF16).astype(F32)
        lined_low = lined - lined_high
        for i, (g, whole, kinds) in enumerate(pieces):
            if whole:
                scatter(i, project([3 * h + k for h in range(2) for k in kinds], g))
        for g in range(1, groups):
            give(g)
        for g in range(groups):
            own.append(project([3 * core + k for k in halves[g]], g))
        for g in range(groups):
            pairs[g].wait_recv()
            both = own[g] + drecv[b, g, :, 0 : len(halves[g]) * wide].astype(F32)
            for i, (g_at, whole, kinds) in enumerate(pieces):
                if g_at == g and not whole:
                    at = halves[g].index(kinds[0]) * wide
                    scatter(i, both[:, at : at + len(kinds) * wide])
        for i in range(len(pieces)):
            zrecv[i][b, 0, core] = zsend[i][b, dp]
        if b > 0:
            split_states(b)
        fade_b = slot_major(fade_ref[:, b, :])
        fade_b = jnp.concatenate([fade_b, jnp.zeros((PAD - rows, heads), F32)], axis=0)
        row_scale = None

        gathered, later = [], []
        for g in range(groups):
            values = {}

            def arrive(slot):
                nonlocal row_scale
                i = next(
                    i
                    for i, (g_at, whole, kinds) in enumerate(pieces)
                    if g_at == g and slot % 3 in kinds
                )
                whole, kinds = pieces[i][1:]
                tiles, extra = piece_shape(pieces[i], per_proj)
                for way in reversed(scattered[i]):
                    way.wait_recv()
                sums = []
                for h in range(2):
                    total = zrecv[i][b, 0, h].astype(F32)
                    for dz in range(1, nz):
                        total = total + zrecv[i][b, dz, h].astype(F32)
                    sums.append(total)
                named = [[3 * h + k for k in kinds] for h in range(2)]
                if whole:
                    sums, named = [sums[0] + sums[1]], [named[0] + named[1]]
                for total, names in zip(sums, named):
                    total, noted = unpack(total, tiles, rows, extra)
                    if noted:
                        line = sum(noted[1:], noted[0])
                        total_squares = jnp.sum(
                            jnp.where(on_row[0:PAD], line, 0.0), axis=1, keepdims=True
                        )
                        row_scale = lax.rsqrt(total_squares / (feats * n_dp) + NORM_EPS)
                    for n, name in enumerate(names):
                        values[name] = total[:, n * wide : (n + 1) * wide] * row_scale

            def flat(slot):
                if slot not in values:
                    arrive(slot)
                return values[slot]

            def by_head(slot):
                rows_now = flat(slot)
                return jnp.stack(
                    [rows_now[:, h * size : (h + 1) * size] for h in range(together)]
                )

            def slots(values):
                return [values[:, t * seqs : (t + 1) * seqs, :] for t in range(steps)]

            key3, fade3 = by_head(0), by_head(3)
            ceiling = ceiling_ref[b : b + 1, g * wide : (g + 1) * wide]
            decay3 = jnp.stack(
                [
                    jnp.exp(
                        fade_b[:, g * together + h : g * together + h + 1]
                        - ceiling[:, h * size : (h + 1) * size] * jax.nn.sigmoid(fade3[h])
                    )
                    for h in range(together)
                ]
            )
            unit3 = key3 * lax.rsqrt(jnp.sum(key3 * key3, axis=2, keepdims=True) + KEY_EPS)
            key, decay, unit = slots(key3), slots(decay3), slots(unit3)
            read = slots(by_head(1))

            wanted = []
            before = None
            for t in range(steps):
                wanted.append(unit[t] if before is None else before * unit[t])
                before = decay[t] if before is None else before * decay[t]
                wanted.append(before * read[t])
            wanted = jnp.concatenate(wanted + filler, axis=1).reshape(together * deep, size)
            wanted_high = wanted.astype(BF16).astype(F32)
            lhs = jnp.concatenate(
                [wanted_high, wanted - wanted_high, wanted_high], axis=1
            ).astype(BF16)
            found = None
            for s in range(seqs):
                product = lax.dot_general(
                    lhs,
                    s_cat[b, s, g * wide : (g + 1) * wide, :],
                    (((1,), (1,)), ((), ())),
                    preferred_element_type=F32,
                )
                found = product if found is None else jnp.where(kind_at == s, product, found)
            found3 = jnp.stack(
                [
                    found[h * deep : (h + 1) * deep, h * size : (h + 1) * size]
                    for h in range(together)
                ]
            )
            pull = slots(unit3 * jax.nn.sigmoid(by_head(4)))
            value = slots(by_head(2))
            base = [found3[:, i * seqs : (i + 1) * seqs, :] for i in range(2 * steps)]

            def dot3(a, c):
                return jnp.sum(a * c, axis=2, keepdims=True)

            taken = []

            def state_times(count, start, vector):
                total = start
                for i in range(count - 1, -1, -1):
                    total = (
                        total - dot3(pull[i], vector) * taken[i] + dot3(key[i], vector) * value[i]
                    )
                    if i:
                        vector = decay[i] * vector
                return total

            readouts = []
            for t in range(steps):
                taken.append(state_times(t, base[2 * t], unit[t]))
                readouts.append(state_times(t + 1, base[2 * t + 1], read[t]))
            readout = jnp.concatenate(readouts, axis=1)
            centered = readout - jnp.mean(readout, axis=2, keepdims=True)
            normed = centered * lax.rsqrt(
                jnp.mean(centered * centered, axis=2, keepdims=True) + GROUP_EPS
            )
            normed_rows = jnp.concatenate([normed[h] for h in range(together)], axis=1)
            gate = jax.nn.sigmoid(flat(5)[0:rows])
            rescale = rescale_ref[b : b + 1, g * wide : (g + 1) * wide]
            mixed = normed_rows * rescale * gate * live_col[0:rows]
            mixed = jnp.concatenate([mixed, jnp.zeros((PAD - rows, wide), F32)], axis=0)
            mbuf[b, g, dp] = mixed.astype(BF16)
            ways = []
            for dz, f in far_first:
                to = dp_to(dz, f)
                ways.append(
                    remote(mbuf.at[b, g, dp], mbuf.at[b, g, dp], peer(tp, to), mbuf.at[b, g, to])
                )
            gathered.append(ways)
            later.append((taken, value, pull, key, decay))

        for g in range(groups):
            taken, value, pull, key, decay = later[g]
            left, right = [], []
            after = None
            for t in range(steps - 1, -1, -1):
                left += [-taken[t] * live3[t], value[t] * live3[t]]
                right += [pull[t] if after is None else pull[t] * after]
                right += [key[t] if after is None else key[t] * after]
                kept = jnp.where(live3[t] > 0.0, decay[t], 1.0)
                after = kept if after is None else after * kept
            left = jnp.concatenate(left + filler, axis=1)
            right = jnp.concatenate(right + filler, axis=1)
            left_high = left.astype(BF16).astype(F32)
            right_high = right.astype(BF16).astype(F32)
            left = jnp.concatenate([left_high, left - left_high, left_high], axis=1).astype(BF16)
            right = jnp.concatenate([right_high, right_high, right - right_high], axis=1)
            for s in range(seqs):
                for h in range(together):
                    at = g * together + h
                    mine = jnp.where(slot_at == s, right[h], 0.0).astype(BF16)
                    state_ref[b, s, at] = mem[b, s, at] * after[h, s : s + 1, :] + lax.dot_general(
                        left[h], mine, (((0,), (0,)), ((), ())), preferred_element_type=F32
                    )

        loads[("e", b)].wait()
        if b < blocks - 1:
            for p in range(6):
                loads[("w", b + 1, p)].wait()
        part = None
        for g in range(groups):
            for way in reversed(gathered[g]):
                way.wait_recv()
            lhs = mbuf[b, g].astype(F32).reshape(n_dp * PAD, wide).astype(BF16)
            product = jnp.dot(
                lhs, ev[b, g * wide : (g + 1) * wide, :], preferred_element_type=F32
            )
            part = product if part is None else part + product
        for j in range(n_dp):
            block = part[j * PAD : (j + 1) * PAD]
            tiles = [block[:, t * LANES : (t + 1) * LANES] for t in range(feat_tiles)]
            psend[b, j] = pack(tiles, rows, []).astype(BF16)
        shared = []
        if b < blocks - 1:
            for i, m in enumerate(tp_offsets):
                shared.append(remote(psend.at[b], precv.at[b, i], peer(tp_to(m), dp)))
            for copy in shared:
                copy.wait_recv()
            for j in range(n_dp):
                at = j * PAD
                total = precv[b, 0, j].astype(F32)
                for i in range(1, n_tp - 1):
                    total = total + precv[b, i, j].astype(F32)
                total, extra = unpack(total, feat_tiles, rows, 0)
                total = total + part[at : at + PAD]
                xs[at : at + PAD, :] = (x_now[at : at + PAD] + total).astype(BF16).astype(F32)
        else:
            pown[...] = x_now + part
            for i, m in enumerate(tp_offsets):
                to = tp_to(m)
                shared.append(
                    remote(
                        psend.at[b, pl.ds(to * per_tp, per_tp)],
                        precv.at[b, i, pl.ds(0, per_tp)],
                        peer(to, dp),
                    )
                )
            for copy in shared:
                copy.wait_recv()
            pieces = []
            for g in range(per_tp):
                at = pl.multiple_of((tp * per_tp + g) * PAD, PAD)
                total = precv[b, 0, g].astype(F32)
                for i in range(1, n_tp - 1):
                    total = total + precv[b, i, g].astype(F32)
                total, extra = unpack(total, feat_tiles, rows, 0)
                pieces.append(sequence_major((pown[pl.ds(at, PAD), :] + total)[0:rows]))
            out_ref[...] = jnp.concatenate(pieces, axis=0).astype(BF16)

    for copy in outgoing:
        copy.wait_send()


def store_kernel(out_vmem, state_vmem, out_hbm, state_hbm, sem):
    copies = [
        pltpu.make_async_copy(state_vmem, state_hbm, sem.at[0]),
        pltpu.make_async_copy(out_vmem, out_hbm, sem.at[1]),
    ]
    for copy in copies:
        copy.start()
    for copy in copies:
        copy.wait()


def solution(mesh):
    n_tp, n_dp = mesh.shape["tp"], mesh.shape["dp"]

    def shards(
        hidden,
        live,
        gain,
        w0,
        w1,
        w2,
        w3,
        w4,
        w5,
        ceiling,
        rescale,
        exit_w,
        memories,
        fade,
    ):
        blocks, feats, chans = w0.shape
        seqs, heads, size = memories.shape[1], memories.shape[2], memories.shape[3]
        rows = fade.shape[1]
        nz = n_dp // 2
        together = max(d for d in range(1, heads + 1) if heads % d == 0 and d * size <= WIDEST)
        groups, wide = heads // together, together * size
        pieces = pieces_of(groups)
        shapes = [piece_shape(piece, wide // LANES) for piece in pieces]
        packed = [LANES * packing(tiles, rows, extra)[0] for tiles, extra in shapes]
        sent = LANES * packing(feats // LANES, rows, 0)[0]
        copies = (n_tp - 1) * (1 + blocks) + blocks * groups
        copies += blocks * (groups + len(pieces)) * (n_dp - 1)
        outputs = 4 * blocks * seqs * heads * size * (-(-size // LANES) * LANES)
        outputs += 4 * hidden.shape[0] * hidden.shape[1]
        vmem = pl.BlockSpec(memory_space=pltpu.VMEM)
        smem = pl.BlockSpec(memory_space=pltpu.SMEM)
        hbm = pl.BlockSpec(memory_space=pl.ANY)
        placed = pl.pallas_call(
            functools.partial(kernel, n_tp, n_dp),
            out_shape=(
                pltpu.VMEM(hidden.shape, hidden.dtype),
                pltpu.VMEM(memories.shape, memories.dtype),
            ),
            in_specs=[hbm, smem] + [hbm] * 12,
            out_specs=(vmem, vmem),
            scratch_shapes=[
                pltpu.VMEM((blocks, 6, feats, chans), BF16),
                pltpu.VMEM((blocks, chans, feats), BF16),
                pltpu.VMEM((blocks, seqs, heads, size, size), F32),
                pltpu.VMEM((n_tp,) + hidden.shape, BF16),
                pltpu.VMEM((n_dp * PAD, feats), F32),
                pltpu.VMEM((n_dp * PAD, feats), F32),
                pltpu.VMEM((blocks, groups, n_dp * PAD, 3 * wide), BF16),
                pltpu.VMEM((blocks, groups, n_dp * PAD, 3 * wide), BF16),
                pltpu.VMEM((blocks, groups, n_dp, PAD, wide), BF16),
                pltpu.VMEM((blocks, n_dp, PAD, sent), BF16),
                pltpu.VMEM((blocks, n_tp - 1, n_dp, PAD, sent), BF16),
                pltpu.VMEM(gain.shape, BF16),
                pltpu.VMEM(ceiling.shape, F32),
                pltpu.VMEM(rescale.shape, F32),
                pltpu.VMEM((rows, blocks, fade.shape[2]), F32),
                pltpu.VMEM((blocks, seqs, heads * size, 3 * size), BF16),
                pltpu.SemaphoreType.DMA((blocks * 8 + 5,)),
                pltpu.SemaphoreType.DMA((copies,)),
                pltpu.SemaphoreType.DMA((copies,)),
            ]
            + [
                pltpu.VMEM((blocks,) + shape + (PAD, width), BF16)
                for width in packed
                for shape in ((n_dp,), (nz, 2))
            ],
            compiler_params=pltpu.CompilerParams(
                collective_id=0, has_side_effects=True, vmem_limit_bytes=VMEM_BYTES - outputs
            ),
        )(hidden, live, gain, w0, w1, w2, w3, w4, w5, ceiling, rescale, exit_w, memories, fade.transpose(1, 0, 2))
        return pl.pallas_call(
            store_kernel,
            out_shape=(
                jax.ShapeDtypeStruct(hidden.shape, hidden.dtype),
                jax.ShapeDtypeStruct(memories.shape, memories.dtype),
            ),
            in_specs=[vmem, vmem],
            out_specs=(hbm, hbm),
            scratch_shapes=[pltpu.SemaphoreType.DMA((2,))],
            compiler_params=pltpu.CompilerParams(vmem_limit_bytes=1048576),
        )(*placed)

    in_specs = (
        P("tp", "dp"),
        P("dp"),
        P(None, "dp"),
        P(None, "dp", "tp"),
        P(None, "dp", "tp"),
        P(None, "dp", "tp"),
        P(None, "dp", "tp"),
        P(None, "dp", "tp"),
        P(None, "dp", "tp"),
        P(None, "tp"),
        P(None, "tp"),
        P(None, "tp", "dp"),
        P(None, "dp", "tp", None, None),
        P(None, "dp", "tp"),
    )
    out_specs = (P("tp", "dp"), P(None, "dp", "tp", None, None))
    return jax.shard_map(shards, mesh=mesh, in_specs=in_specs, out_specs=out_specs, check_vma=False)
```

time: 47.5 us -> 42.9 us (0.903)
  Pallas kernels: 46.6 us -> 42 us
    pallas_call x1, Pallas kernels: 45.4 us -> 40.9 us  [shards(): pl.pallas_call(functools.partial(kernel, n_tp, n_dp), out_shape=(pltpu.VM...]
where the time goes in v3:
time: 42.9 us; the launch traced here: 42.7 us
  Pallas kernels  42 us (98%)
  between operations  0.64 us (1%)
    pallas_call x1, Pallas kernels, shards(): pl.pallas_call(functools.partial(kernel, n_tp, n_dp), out_shape=(pltpu.VM...  40.9 us
    pallas_call x1, Pallas kernels, shards(): pl.pallas_call(store_kernel, out_shape=(jax.ShapeDtypeStruct(hidden.shape...  1.16 us

profile of v3, /device:TPU:0, one launch (start us, length us, event | category | flops | bytes accessed | tf_op | source)
XLA Modules:
  0.0 42.7 jit_solution(10248294469736421944)
XLA Ops:
  0.6 40.9 %shard_map.149 = (bf16[12,512]{1,0:T(8,128)(2,1)S(1)}, f32[2,3,8,64,64]{4,3,2,1,0:T(8,128)S(1)}) custom-call(bf16[12,512]{1,0:T(8,128)(2,1)} %x_hbm.1, s32[3]{0:T(128)} %live_ref.1, bf16[2,512]{1,0:T(2,128)(2,1)} %gain_hbm.1, bf16[2,512,512]{2,1,0:T(8,128)(2,1)} %w0.1, bf16[2,512,512]{2,1,0:T(8,128)(2,1)} %w1.1, bf16[2,512,512]{2,1,0:T(8,128)(2,1)} %w2.1, ...), custom_call_target="tpu_custom_call" | custom-call | tf_op jit(solution)/shard_map/pallas_call | solution.py:631
  41.5 1.2 %shard_map.150 = (bf16[12,512]{1,0:T(8,128)(2,1)}, f32[2,3,8,64,64]{4,3,2,1,0:T(8,128)}) custom-call(bf16[12,512]{1,0:T(8,128)(2,1)S(1)} %get-tuple-element.4.out_vmem, f32[2,3,8,64,64]{4,3,2,1,0:T(8,128)S(1)} %get-tuple-element.5.state_vmem), custom_call_target="tpu_custom_call" | custom-call | tf_op jit(solution)/shard_map/pallas_call | solution.py:669

commit v4 on v3

--- a/solution.py
+++ b/solution.py
@@ -80,7 +80,7 @@
 
 def piece_shape(piece, per_proj):
     g, whole, kinds = piece
-    return len(kinds) * per_proj * (2 if whole else 1), 2 if whole else 0
+    return len(kinds) * per_proj * (2 if whole else 1)
 
 
 def kernel(
@@ -113,6 +113,8 @@
     mbuf,
     psend,
     precv,
+    qsend,
+    qrecv,
     gain_ref,
     ceiling_ref,
     rescale_ref,
@@ -135,7 +137,9 @@
     per_proj = wide // LANES
     pieces = pieces_of(groups)
     zsend, zrecv = piece_refs[0::2], piece_refs[1::2]
-    feat_tiles = feats // LANES
+    cuts, dests = psend.shape[1], n_dp // psend.shape[2]
+    cut_feats = feats // cuts
+    cut_tiles = cut_feats // LANES
 
     tp = lax.axis_index("tp")
     dp = lax.axis_index("dp")
@@ -154,12 +158,12 @@
             bit *= 2
         return at
 
-    def dp_to(dz, flip):
-        return lax.rem(z + dz, nz) * 2 + (other if flip else core)
+    sibling = z * 2 + other
+    far = [sorted(range(nz), key=lambda at: -abs(at - i)) for i in range(nz)]
+    far_z = [sum(jnp.where(z == i, far[i][k], 0) for i in range(nz)) for k in range(nz - 1)]
+    dp_others = [at * 2 + c for at in far_z for c in (core, other)] + [sibling]
 
     tp_offsets = sorted(range(1, n_tp), key=lambda m: -bin(m).count("1"))
-    dp_offsets = [(dz, f) for dz in range(nz) for f in range(2) if (dz, f) != (0, 0)]
-    far_first = sorted(dp_offsets, key=lambda o: -min(o[0], nz - o[0]))
 
     def slot_major(values):
         return jnp.concatenate(
@@ -202,7 +206,33 @@
         outgoing.append(sent)
         return sent if lands is None else copy(lands)
 
+    def spread(src_for, dst_of):
+        at = counter[0]
+        counter[0] += n_dp
+
+        def copy(k, to, dst_ref, source):
+            return pltpu.make_async_remote_copy(
+                src_ref=src_for(to),
+                dst_ref=dst_ref,
+                send_sem=send_sem.at[at + k],
+                recv_sem=recv_sem.at[at + source],
+                device_id=peer(tp, to),
+                device_id_type=pl.DeviceIdType.MESH,
+            )
+
+        for k, to in enumerate(dp_others):
+            sent = copy(k, to, dst_of(dp), dp)
+            sent.start()
+            outgoing.append(sent)
+        return [copy(k, to, dst_of(to), to) for k, to in enumerate(dp_others)]
+
     outgoing = []
+
+    def flush(count):
+        for copy in outgoing[:count]:
+            copy.wait_send()
+        del outgoing[:count]
+
     weights = (w1, w0, w2, w3, w4, w5)
     loads = {}
 
@@ -212,6 +242,15 @@
         loads[name] = copy
 
     load("x", x_hbm, gx.at[tp])
+    barrier = pltpu.get_barrier_semaphore()
+    for m in tp_offsets:
+        pl.semaphore_signal(
+            barrier, inc=1, device_id=peer(tp_to(m), dp), device_id_type=pl.DeviceIdType.MESH
+        )
+    for to in dp_others:
+        pl.semaphore_signal(
+            barrier, inc=1, device_id=peer(tp, to), device_id_type=pl.DeviceIdType.MESH
+        )
     load("gain", gain_hbm, gain_ref)
     load("ceiling", ceiling_hbm, ceiling_ref)
     load("rescale", rescale_hbm, rescale_ref)
@@ -222,18 +261,9 @@
         load(("m", b), memory_hbm.at[b], mem.at[b])
         load(("e", b), exit_hbm.at[b], ev.at[b])
 
-    barrier = pltpu.get_barrier_semaphore()
-    for m in tp_offsets:
-        pl.semaphore_signal(
-            barrier, inc=1, device_id=peer(tp_to(m), dp), device_id_type=pl.DeviceIdType.MESH
-        )
-    for dz, f in far_first:
-        pl.semaphore_signal(
-            barrier, inc=1, device_id=peer(tp, dp_to(dz, f)), device_id_type=pl.DeviceIdType.MESH
-        )
     xs[...] = jnp.zeros_like(xs)
     loads["x"].wait()
-    pl.semaphore_wait(barrier, n_tp - 1 + len(dp_offsets))
+    pl.semaphore_wait(barrier, n_tp - 1 + len(dp_others))
 
     first = []
     for m in tp_offsets:
@@ -283,6 +313,28 @@
             )
 
     for b in range(blocks):
+        older = len(outgoing)
+
+        def settle(c):
+            for copy in shared[c]:
+                copy.wait_recv()
+            lanes = slice(c * cut_feats, (c + 1) * cut_feats)
+            for i in range(n_dp // dests):
+                total = precv[b - 1, 0, c, i].astype(F32)
+                for k in range(1, n_tp - 1):
+                    total = total + precv[b - 1, k, c, i].astype(F32)
+                total, extra = unpack(total, dests * cut_tiles, rows, 0)
+                for k in range(dests):
+                    at = (i * dests + k) * PAD
+                    mine = total[:, k * cut_feats : (k + 1) * cut_feats]
+                    mine = mine + part[c][at : at + PAD]
+                    xs[at : at + PAD, lanes] = (
+                        (xs[at : at + PAD, lanes] + mine).astype(BF16).astype(F32)
+                    )
+
+        if b > 0:
+            for c in range(cuts):
+                settle(c)
         x_now = xs[...]
         gained = (x_now * gain_ref[b : b + 1, :].astype(F32)).astype(BF16)
 
@@ -302,24 +354,12 @@
         scattered = {}
 
         def scatter(i, values):
-            tiles, extra = piece_shape(pieces[i], per_proj)
+            tiles = piece_shape(pieces[i], per_proj)
             for j in range(n_dp):
                 block = values[j * PAD : (j + 1) * PAD]
                 cut = [block[:, t * LANES : (t + 1) * LANES] for t in range(tiles)]
-                noted = [lined_high[j : j + 1], lined_low[j : j + 1]] if extra else []
-                zsend[i][b, j] = pack(cut, rows, noted).astype(BF16)
-            ways = []
-            for dz, f in far_first:
-                to = dp_to(dz, f)
-                ways.append(
-                    remote(
-                        zsend[i].at[b, to],
-                        zrecv[i].at[b, dz, core],
-                        peer(tp, to),
-                        zrecv[i].at[b, dz, other if f else core],
-                    )
-                )
-            scattered[i] = ways
+                zsend[i][b, j] = pack(cut, rows, []).astype(BF16)
+            scattered[i] = spread(lambda to: zsend[i].at[b, to], lambda at: zrecv[i].at[b, at])
 
         halves = [
             sorted(k for g_at, whole, kinds in pieces if g_at == g and not whole for k in kinds)
@@ -327,41 +367,52 @@
         ]
         pairs, own = [], []
 
-        def give(g):
+        def give(g, values):
             width = len(halves[g]) * wide
-            dsend[b, g, :, 0:width] = project([3 * other + k for k in halves[g]], g).astype(BF16)
+            dsend[b, g, :, 0:width] = values.astype(BF16)
             pairs.append(
                 remote(
                     dsend.at[b, g, :, pl.ds(0, width)],
                     drecv.at[b, g, :, pl.ds(0, width)],
-                    peer(tp, dp_to(0, 1)),
+                    peer(tp, sibling),
                 )
             )
 
-        give(0)
+        def theirs(g):
+            return [3 * other + k for k in halves[g]]
+
+        reduced = [g for g in range(groups) if halves[g]]
+        give(0, project(theirs(0), 0))
         squares = jnp.sum(x_now * x_now, axis=1, keepdims=True)
         lined = jnp.where(on_row, squares, 0.0).reshape(n_dp, PAD, LANES)
         lined = jnp.sum(lined, axis=1)
         lined_high = lined.astype(BF16).astype(F32)
         lined_low = lined - lined_high
+        for j in range(n_dp):
+            qsend[b, j] = jnp.where(
+                row_at == 0, lined_high[j : j + 1], lined_low[j : j + 1]
+            ).astype(BF16)
+        noted = spread(lambda to: qsend.at[b, to], lambda at: qrecv.at[b, at])
         for i, (g, whole, kinds) in enumerate(pieces):
             if whole:
                 scatter(i, project([3 * h + k for h in range(2) for k in kinds], g))
-        for g in range(1, groups):
-            give(g)
-        for g in range(groups):
+        for g in reduced[1:]:
+            give(g, project(theirs(g), g))
+        for n, g in enumerate(reduced):
             own.append(project([3 * core + k for k in halves[g]], g))
-        for g in range(groups):
-            pairs[g].wait_recv()
-            both = own[g] + drecv[b, g, :, 0 : len(halves[g]) * wide].astype(F32)
+            pairs[n].wait_recv()
+            both = own[n] + drecv[b, g, :, 0 : len(halves[g]) * wide].astype(F32)
             for i, (g_at, whole, kinds) in enumerate(pieces):
                 if g_at == g and not whole:
                     at = halves[g].index(kinds[0]) * wide
                     scatter(i, both[:, at : at + len(kinds) * wide])
         for i in range(len(pieces)):
-            zrecv[i][b, 0, core] = zsend[i][b, dp]
+            zrecv[i][b, dp] = zsend[i][b, dp]
+        qrecv[b, dp] = qsend[b, dp]
         if b > 0:
             split_states(b)
+        flush(older)
+        spent = len(outgoing)
         fade_b = slot_major(fade_ref[:, b, :])
         fade_b = jnp.concatenate([fade_b, jnp.zeros((PAD - rows, heads), F32)], axis=0)
         row_scale = None
@@ -378,26 +429,31 @@
                     if g_at == g and slot % 3 in kinds
                 )
                 whole, kinds = pieces[i][1:]
-                tiles, extra = piece_shape(pieces[i], per_proj)
+                tiles = piece_shape(pieces[i], per_proj)
+                if row_scale is None:
+                    for way in reversed(noted):
+                        way.wait_recv()
+                    line = qrecv[b, 0].astype(F32)
+                    for at in range(1, n_dp):
+                        line = line + qrecv[b, at].astype(F32)
+                    line = line[0:1] + line[1:2]
+                    total_squares = jnp.sum(
+                        jnp.where(on_row[0:PAD], line, 0.0), axis=1, keepdims=True
+                    )
+                    row_scale = lax.rsqrt(total_squares / (feats * n_dp) + NORM_EPS)
                 for way in reversed(scattered[i]):
                     way.wait_recv()
                 sums = []
                 for h in range(2):
-                    total = zrecv[i][b, 0, h].astype(F32)
-                    for dz in range(1, nz):
-                        total = total + zrecv[i][b, dz, h].astype(F32)
+                    total = zrecv[i][b, h].astype(F32)
+                    for at in range(1, nz):
+                        total = total + zrecv[i][b, 2 * at + h].astype(F32)
                     sums.append(total)
                 named = [[3 * h + k for k in kinds] for h in range(2)]
                 if whole:
                     sums, named = [sums[0] + sums[1]], [named[0] + named[1]]
                 for total, names in zip(sums, named):
-                    total, noted = unpack(total, tiles, rows, extra)
-                    if noted:
-                        line = sum(noted[1:], noted[0])
-                        total_squares = jnp.sum(
-                            jnp.where(on_row[0:PAD], line, 0.0), axis=1, keepdims=True
-                        )
-                        row_scale = lax.rsqrt(total_squares / (feats * n_dp) + NORM_EPS)
+                    total, extra = unpack(total, tiles, rows, 0)
                     for n, name in enumerate(names):
                         values[name] = total[:, n * wide : (n + 1) * wide] * row_scale
 
@@ -457,28 +513,31 @@
                 ]
             )
             pull = slots(unit3 * jax.nn.sigmoid(by_head(4)))
-            value = slots(by_head(2))
             base = [found3[:, i * seqs : (i + 1) * seqs, :] for i in range(2 * steps)]
 
             def dot3(a, c):
                 return jnp.sum(a * c, axis=2, keepdims=True)
 
-            taken = []
-
-            def state_times(count, start, vector):
-                total = start
+            def weigh(count, vector):
+                pairs = []
                 for i in range(count - 1, -1, -1):
-                    total = (
-                        total - dot3(pull[i], vector) * taken[i] + dot3(key[i], vector) * value[i]
-                    )
+                    pairs.append((i, dot3(pull[i], vector), dot3(key[i], vector)))
                     if i:
                         vector = decay[i] * vector
-                return total
-
-            readouts = []
+                return pairs
+
+            weighed = [(weigh(t, unit[t]), weigh(t + 1, read[t])) for t in range(steps)]
+            value = slots(by_head(2))
+            taken, readouts = [], []
+
+            def state_times(start, pairs):
+                for i, pulled, keyed in pairs:
+                    start = start - pulled * taken[i] + keyed * value[i]
+                return start
+
             for t in range(steps):
-                taken.append(state_times(t, base[2 * t], unit[t]))
-                readouts.append(state_times(t + 1, base[2 * t + 1], read[t]))
+                taken.append(state_times(base[2 * t], weighed[t][0]))
+                readouts.append(state_times(base[2 * t + 1], weighed[t][1]))
             readout = jnp.concatenate(readouts, axis=1)
             centered = readout - jnp.mean(readout, axis=2, keepdims=True)
             normed = centered * lax.rsqrt(
@@ -490,102 +549,114 @@
             mixed = normed_rows * rescale * gate * live_col[0:rows]
             mixed = jnp.concatenate([mixed, jnp.zeros((PAD - rows, wide), F32)], axis=0)
             mbuf[b, g, dp] = mixed.astype(BF16)
-            ways = []
-            for dz, f in far_first:
-                to = dp_to(dz, f)
-                ways.append(
-                    remote(mbuf.at[b, g, dp], mbuf.at[b, g, dp], peer(tp, to), mbuf.at[b, g, to])
-                )
-            gathered.append(ways)
+            gathered.append(
+                spread(lambda to: mbuf.at[b, g, dp], lambda at: mbuf.at[b, g, at])
+            )
             later.append((taken, value, pull, key, decay))
 
-        for g in range(groups):
-            taken, value, pull, key, decay = later[g]
-            left, right = [], []
-            after = None
-            for t in range(steps - 1, -1, -1):
-                left += [-taken[t] * live3[t], value[t] * live3[t]]
-                right += [pull[t] if after is None else pull[t] * after]
-                right += [key[t] if after is None else key[t] * after]
-                kept = jnp.where(live3[t] > 0.0, decay[t], 1.0)
-                after = kept if after is None else after * kept
-            left = jnp.concatenate(left + filler, axis=1)
-            right = jnp.concatenate(right + filler, axis=1)
-            left_high = left.astype(BF16).astype(F32)
-            right_high = right.astype(BF16).astype(F32)
-            left = jnp.concatenate([left_high, left - left_high, left_high], axis=1).astype(BF16)
-            right = jnp.concatenate([right_high, right_high, right - right_high], axis=1)
-            for s in range(seqs):
-                for h in range(together):
-                    at = g * together + h
-                    mine = jnp.where(slot_at == s, right[h], 0.0).astype(BF16)
-                    state_ref[b, s, at] = mem[b, s, at] * after[h, s : s + 1, :] + lax.dot_general(
-                        left[h], mine, (((0,), (0,)), ((), ())), preferred_element_type=F32
-                    )
-
+        @pl.when(core >= 0)
+        def _():
+            for g in range(groups):
+                taken, value, pull, key, decay = later[g]
+                left, right = [], []
+                after = None
+                for t in range(steps - 1, -1, -1):
+                    left += [-taken[t] * live3[t], value[t] * live3[t]]
+                    right += [pull[t] if after is None else pull[t] * after]
+                    right += [key[t] if after is None else key[t] * after]
+                    kept = jnp.where(live3[t] > 0.0, decay[t], 1.0)
+                    after = kept if after is None else after * kept
+                left = jnp.concatenate(left + filler, axis=1)
+                right = jnp.concatenate(right + filler, axis=1)
+                left_high = left.astype(BF16).astype(F32)
+                right_high = right.astype(BF16).astype(F32)
+                left = jnp.concatenate([left_high, left - left_high, left_high], axis=1).astype(BF16)
+                right = jnp.concatenate([right_high, right_high, right - right_high], axis=1)
+                for s in range(seqs):
+                    for h in range(together):
+                        at = g * together + h
+                        mine = jnp.where(slot_at == s, right[h], 0.0).astype(BF16)
+                        state_ref[b, s, at] = mem[b, s, at] * after[h, s : s + 1, :] + lax.dot_general(
+                            left[h], mine, (((0,), (0,)), ((), ())), preferred_element_type=F32
+                        )
+
+        flush(spent)
         loads[("e", b)].wait()
         if b < blocks - 1:
             for p in range(6):
                 loads[("w", b + 1, p)].wait()
-        part = None
+        every = None
         for g in range(groups):
             for way in reversed(gathered[g]):
                 way.wait_recv()
-            lhs = mbuf[b, g].astype(F32).reshape(n_dp * PAD, wide).astype(BF16)
+            mixed_rows = mbuf[b, g].astype(F32).reshape(n_dp * PAD, wide).astype(BF16)
             product = jnp.dot(
-                lhs, ev[b, g * wide : (g + 1) * wide, :], preferred_element_type=F32
-            )
-            part = product if part is None else part + product
-        for j in range(n_dp):
-            block = part[j * PAD : (j + 1) * PAD]
-            tiles = [block[:, t * LANES : (t + 1) * LANES] for t in range(feat_tiles)]
-            psend[b, j] = pack(tiles, rows, []).astype(BF16)
-        shared = []
-        if b < blocks - 1:
-            for i, m in enumerate(tp_offsets):
-                shared.append(remote(psend.at[b], precv.at[b, i], peer(tp_to(m), dp)))
-            for copy in shared:
-                copy.wait_recv()
-            for j in range(n_dp):
-                at = j * PAD
-                total = precv[b, 0, j].astype(F32)
-                for i in range(1, n_tp - 1):
-                    total = total + precv[b, i, j].astype(F32)
-                total, extra = unpack(total, feat_tiles, rows, 0)
-                total = total + part[at : at + PAD]
-                xs[at : at + PAD, :] = (x_now[at : at + PAD] + total).astype(BF16).astype(F32)
-        else:
-            pown[...] = x_now + part
-            for i, m in enumerate(tp_offsets):
-                to = tp_to(m)
+                mixed_rows, ev[b, g * wide : (g + 1) * wide], preferred_element_type=F32
+            )
+            every = product if every is None else every + product
+        part, shared = [], []
+        for c in range(cuts):
+            value = every[:, c * cut_feats : (c + 1) * cut_feats]
+            part.append(value)
+            for i in range(n_dp // dests):
+                cut = [
+                    value[at * PAD : (at + 1) * PAD, t * LANES : (t + 1) * LANES]
+                    for at in range(i * dests, (i + 1) * dests)
+                    for t in range(cut_tiles)
+                ]
+                psend[b, c, i] = pack(cut, rows, []).astype(BF16)
+            if b < blocks - 1:
                 shared.append(
-                    remote(
-                        psend.at[b, pl.ds(to * per_tp, per_tp)],
-                        precv.at[b, i, pl.ds(0, per_tp)],
-                        peer(to, dp),
-                    )
+                    [
+                        remote(psend.at[b, c], precv.at[b, k, c], peer(tp_to(m), dp))
+                        for k, m in enumerate(tp_offsets)
+                    ]
                 )
-            for copy in shared:
-                copy.wait_recv()
-            pieces = []
-            for g in range(per_tp):
-                at = pl.multiple_of((tp * per_tp + g) * PAD, PAD)
-                total = precv[b, 0, g].astype(F32)
-                for i in range(1, n_tp - 1):
-                    total = total + precv[b, i, g].astype(F32)
-                total, extra = unpack(total, feat_tiles, rows, 0)
-                pieces.append(sequence_major((pown[pl.ds(at, PAD), :] + total)[0:rows]))
-            out_ref[...] = jnp.concatenate(pieces, axis=0).astype(BF16)
-
-    for copy in outgoing:
-        copy.wait_send()
+    b = blocks - 1
+    last = []
+    places = per_tp // dests
+    for k, m in enumerate(tp_offsets):
+        to = tp_to(m)
+        last.append(
+            remote(
+                psend.at[b, :, pl.ds(to * places, places)],
+                precv.at[b, k, :, pl.ds(0, places)],
+                peer(to, dp),
+            )
+        )
+    pown[...] = xs[...] + jnp.concatenate(part, axis=1)
+    flush(len(outgoing) - len(last))
+    for copy in last:
+        copy.wait_recv()
+    finished = []
+    for i in range(places):
+        found = []
+        for c in range(cuts):
+            total = precv[b, 0, c, i].astype(F32)
+            for k in range(1, n_tp - 1):
+                total = total + precv[b, k, c, i].astype(F32)
+            found.append(unpack(total, dests * cut_tiles, rows, 0)[0])
+        for k in range(dests):
+            at = pl.multiple_of((tp * per_tp + i * dests + k) * PAD, PAD)
+            total = jnp.concatenate(
+                [f[:, k * cut_feats : (k + 1) * cut_feats] for f in found], axis=1
+            )
+            finished.append(sequence_major((pown[pl.ds(at, PAD), :] + total)[0:rows]))
+    out_ref[...] = jnp.concatenate(finished, axis=0).astype(BF16)
+
+    flush(len(outgoing))
 
 
 def store_kernel(out_vmem, state_vmem, out_hbm, state_hbm, sem):
+    blocks, seqs = state_vmem.shape[0:2]
     copies = [
-        pltpu.make_async_copy(state_vmem, state_hbm, sem.at[0]),
-        pltpu.make_async_copy(out_vmem, out_hbm, sem.at[1]),
+        pltpu.make_async_copy(
+            state_vmem.at[b, i], state_hbm.at[b, i], sem.at[b * seqs + i]
+        )
+        for b in range(blocks)
+        for i in range(seqs)
     ]
+    copies.append(pltpu.make_async_copy(out_vmem, out_hbm, sem.at[blocks * seqs]))
     for copy in copies:
         copy.start()
     for copy in copies:
@@ -614,15 +685,16 @@
         blocks, feats, chans = w0.shape
         seqs, heads, size = memories.shape[1], memories.shape[2], memories.shape[3]
         rows = fade.shape[1]
-        nz = n_dp // 2
         together = max(d for d in range(1, heads + 1) if heads % d == 0 and d * size <= WIDEST)
         groups, wide = heads // together, together * size
         pieces = pieces_of(groups)
         shapes = [piece_shape(piece, wide // LANES) for piece in pieces]
-        packed = [LANES * packing(tiles, rows, extra)[0] for tiles, extra in shapes]
-        sent = LANES * packing(feats // LANES, rows, 0)[0]
-        copies = (n_tp - 1) * (1 + blocks) + blocks * groups
-        copies += blocks * (groups + len(pieces)) * (n_dp - 1)
+        packed = [LANES * packing(tiles, rows, 0)[0] for tiles in shapes]
+        cuts = 1
+        dests = 2 if n_dp // n_tp % 2 == 0 else 1
+        sent = LANES * packing(dests * (feats // cuts // LANES), rows, 0)[0]
+        copies = (n_tp - 1) * (1 + blocks * cuts) + blocks * groups
+        copies += blocks * (1 + groups + len(pieces)) * n_dp
         outputs = 4 * blocks * seqs * heads * size * (-(-size // LANES) * LANES)
         outputs += 4 * hidden.shape[0] * hidden.shape[1]
         vmem = pl.BlockSpec(memory_space=pltpu.VMEM)
@@ -646,8 +718,10 @@
                 pltpu.VMEM((blocks, groups, n_dp * PAD, 3 * wide), BF16),
                 pltpu.VMEM((blocks, groups, n_dp * PAD, 3 * wide), BF16),
                 pltpu.VMEM((blocks, groups, n_dp, PAD, wide), BF16),
-                pltpu.VMEM((blocks, n_dp, PAD, sent), BF16),
-                pltpu.VMEM((blocks, n_tp - 1, n_dp, PAD, sent), BF16),
+                pltpu.VMEM((blocks, cuts, n_dp // dests, PAD, sent), BF16),
+                pltpu.VMEM((blocks, n_tp - 1, cuts, n_dp // dests, PAD, sent), BF16),
+                pltpu.VMEM((blocks, n_dp, PAD, LANES), BF16),
+                pltpu.VMEM((blocks, n_dp, PAD, LANES), BF16),
                 pltpu.VMEM(gain.shape, BF16),
                 pltpu.VMEM(ceiling.shape, F32),
                 pltpu.VMEM(rescale.shape, F32),
@@ -658,9 +732,9 @@
                 pltpu.SemaphoreType.DMA((copies,)),
             ]
             + [
-                pltpu.VMEM((blocks,) + shape + (PAD, width), BF16)
+                pltpu.VMEM((blocks, n_dp, PAD, width), BF16)
                 for width in packed
-                for shape in ((n_dp,), (nz, 2))
+                for _ in range(2)
             ],
             compiler_params=pltpu.CompilerParams(
                 collective_id=0, has_side_effects=True, vmem_limit_bytes=VMEM_BYTES - outputs
@@ -674,7 +748,7 @@
             ),
             in_specs=[vmem, vmem],
             out_specs=(hbm, hbm),
-            scratch_shapes=[pltpu.SemaphoreType.DMA((2,))],
+            scratch_shapes=[pltpu.SemaphoreType.DMA((blocks * seqs + 1,))],
             compiler_params=pltpu.CompilerParams(vmem_limit_bytes=1048576),
         )(*placed)
 

time: 42.9 us -> 42.5 us (level)
    pallas_call x1, Pallas kernels: 40.9 us -> 40.4 us  [shards(): pl.pallas_call(functools.partial(kernel, n_tp, n_dp), out_shape=(pltpu.VM...]
where the time goes in v4:
time: 42.5 us; the launch traced here: 42.2 us
  Pallas kernels  41.6 us (98%)
  between operations  0.64 us (2%)
    pallas_call x1, Pallas kernels, shards(): pl.pallas_call(functools.partial(kernel, n_tp, n_dp), out_shape=(pltpu.VM...  40.4 us
    pallas_call x1, Pallas kernels, shards(): pl.pallas_call(store_kernel, out_shape=(jax.ShapeDtypeStruct(hidden.shape...  1.2 us

profile of v4, /device:TPU:0, one launch (start us, length us, event | category | flops | bytes accessed | tf_op | source)
XLA Modules:
  0.0 42.2 jit_solution(16484096372892458085)
XLA Ops:
  0.6 40.4 %shard_map.149 = (bf16[12,512]{1,0:T(8,128)(2,1)S(1)}, f32[2,3,8,64,64]{4,3,2,1,0:T(8,128)S(1)}) custom-call(bf16[12,512]{1,0:T(8,128)(2,1)} %x_hbm.1, s32[3]{0:T(128)} %live_ref.1, bf16[2,512]{1,0:T(2,128)(2,1)} %gain_hbm.1, bf16[2,512,512]{2,1,0:T(8,128)(2,1)} %w0.1, bf16[2,512,512]{2,1,0:T(8,128)(2,1)} %w1.1, bf16[2,512,512]{2,1,0:T(8,128)(2,1)} %w2.1, ...), custom_call_target="tpu_custom_call" | custom-call | tf_op jit(solution)/shard_map/pallas_call | solution.py:703
  41.0 1.2 %shard_map.150 = (bf16[12,512]{1,0:T(8,128)(2,1)}, f32[2,3,8,64,64]{4,3,2,1,0:T(8,128)}) custom-call(bf16[12,512]{1,0:T(8,128)(2,1)S(1)} %get-tuple-element.4.out_vmem, f32[2,3,8,64,64]{4,3,2,1,0:T(8,128)S(1)} %get-tuple-element.5.state_vmem), custom_call_target="tpu_custom_call" | custom-call | tf_op jit(solution)/shard_map/pallas_call | solution.py:743
